TPU v7x, 32 devices: a whole 2x2x4 slice. The times are simulated.
32 devices in a mesh: gr: 2 (over x), sp: 8 (over z, y), tp: 2 (over core).
Axes of the slice: x: 2, y: 2, z: 4, core: 2. Of those that a mesh axis runs over, the one named last changes fastest.
Arguments:
- tokens: bfloat16 [4, 4096, 2048], P('gr', 'sp'), parts along dimension 0, may hold values from -6 to 6
- key_matrix: bfloat16 [2048, 2048], P(None, 'tp'), may hold values from -0.125 to 0.125
- value_matrix: bfloat16 [2048, 2048], P(None, 'tp'), may hold values from -0.125 to 0.125
- gate_matrix: bfloat16 [2048, 16], replicated, may hold values from -0.125 to 0.125
- decay_matrix: bfloat16 [2048, 16], replicated, may hold values from -0.125 to 0.125
- gate_bias_offset: float32 [16], replicated, may hold values from -8 to 1
- head_log_decay_rate: float32 [16], replicated, may hold values from -12 to -2
- extra_log_decay: float32 [4, 4096, 16], P('gr', 'sp', 'tp'), parts along dimension 0, may hold values from -1 to 0
- next_token_query: bfloat16 [4, 16, 128], P('gr', 'tp'), parts along dimension 0, may hold values from -6 to 6
- next_token_key: bfloat16 [4, 16, 128], P('gr', 'tp'), parts along dimension 0, may hold values from -6 to 6
- next_token_value: bfloat16 [4, 16, 128], P('gr', 'tp'), parts along dimension 0, may hold values from -6 to 6
- next_token_gate: float32 [4, 16], P('gr', 'tp'), parts along dimension 0, may hold values from -2 to 2
- readout_norm_gain: float32 [128], replicated, may hold values from 0.1 to 1.9
Outputs:
- state_cache: bfloat16 [4, 16, 128, 128], P('gr', 'tp', 'sp'), parts along dimension 0
- first_read: bfloat16 [4, 16, 128], P('gr', 'tp'), parts along dimension 0
There are 2 independent parts, one for each index of `gr`. A program takes and returns all parts, laid end to end along the dimension named above; an argument that names none is the same for every part. Nothing has to cross between parts.
All inputs are finite; a program needn't handle non-finite values.
Results may differ from a plain program's by a relative error of at most 0.009.
Values sent between devices are 32-bit elements; how exact they have to be, the bound alone decides.
A program may use at most 64 MiB of HBM per device.

v0:
```python
import functools
import math

import jax
import jax.numpy as jnp
from jax import lax
from jax.experimental import pallas as pl
from jax.experimental.pallas import tpu as pltpu
from jax.sharding import PartitionSpec as P

BLOCK = 64
PACK = 4
EPS = 1e-06
F32 = jnp.float32
BF16 = jnp.bfloat16


def contract(left, right, left_dim, right_dim):
    return lax.dot_general(
        left, right, (((left_dim,), (right_dim,)), ((), ())), preferred_element_type=F32
    )


def dot(left, right):
    return contract(left, right, 1, 0)


def split(array, terms):
    pieces = []
    rest = array
    for _ in range(terms):
        piece = rest.astype(BF16)
        pieces.append(piece)
        rest = rest - piece.astype(F32)
    return pieces


def dot3(left, right):
    left_hi, left_lo = split(left, 2)
    right_hi, right_lo = split(right, 2)
    return dot(left_hi, right_hi) + (dot(left_hi, right_lo) + dot(left_lo, right_hi))


def exact_times_ones(array, ones):
    total = None
    for piece in split(array, 3):
        term = dot(piece, ones)
        total = term if total is None else total + term
    return total


def prepare(tok_ref, wgd_ref, shift_ref, rate_ref, extra_ref, rows_ref, cols_ref, masks_ref):
    heads = shift_ref.shape[0]
    length = tok_ref.shape[0]
    span = PACK * BLOCK
    row = lax.broadcasted_iota(jnp.int32, (span, span), 0)
    col = lax.broadcasted_iota(jnp.int32, (span, span), 1)
    same = (row // BLOCK) == (col // BLOCK)
    level = 0
    size = 2
    while size < BLOCK:
        inside = (row // (2 * size) == col // (2 * size)) & (row // size != col // size) & (row > col)
        masks_ref[level] = jnp.where(inside, 1.0, 0.0).astype(BF16)
        size *= 2
        level += 1
    masks_ref[level] = jnp.where(same, 1.0, 0.0).astype(BF16)
    upper = jnp.where(same & (row <= col), 1.0, 0.0).astype(BF16)
    every = jnp.where(same, 1.0, 0.0).astype(BF16)
    logits = contract(wgd_ref[...], tok_ref[...], 1, 1)
    gate = logits[:heads] + shift_ref[...]
    decay = logits[heads : 2 * heads]
    beta = 1.0 / (1.0 + jnp.exp(-gate))
    soft = jnp.maximum(decay, 0.0) + jnp.log1p(jnp.exp(-jnp.abs(decay)))
    log_decay = -jnp.exp(rate_ref[...]) * soft + extra_ref[...]
    for at in range(length // span):
        lanes = slice(at * span, (at + 1) * span)
        part = log_decay[:, lanes]
        cum = exact_times_ones(part, upper)
        total = exact_times_ones(part, every)
        grow = jnp.exp(cum)
        outward = jnp.exp(total - cum)
        carry = jnp.exp(total)
        b = beta[:, lanes]
        for h in range(heads):
            one = slice(h, h + 1)
            stack = jnp.concatenate(
                [cum[one], b[one], b[one] * grow[one], outward[one], carry[one],
                 cum[one], cum[one], cum[one]],
                axis=0,
            )
            rows_ref[h, :, lanes] = stack
            cols_ref[h, lanes, :] = jnp.transpose(stack)


def pack_terms(keys, values, rows, cols, masks_ref):
    span = PACK * BLOCK
    levels = masks_ref.shape[0] - 1
    row = lax.broadcasted_iota(jnp.int32, (span, span), 0)
    col = lax.broadcasted_iota(jnp.int32, (span, span), 1)
    strict = (row // BLOCK == col // BLOCK) & (row > col)
    cum_col, beta_col, pull_col, out_col = (cols[:, i : i + 1] for i in range(4))
    cum_row = rows[0:1]
    gram = contract(keys, keys, 1, 1)
    scale = jnp.exp(jnp.where(strict, cum_col - cum_row, -1e30))
    lower = (beta_col * gram) * scale
    packed = lower[0:BLOCK]
    for p in range(1, PACK):
        packed = packed + lower[p * BLOCK : (p + 1) * BLOCK]
    lower = lower.astype(BF16)
    prow = lax.broadcasted_iota(jnp.int32, (BLOCK, span), 0)
    pcol = lax.rem(lax.broadcasted_iota(jnp.int32, (BLOCK, span), 1), BLOCK)
    inv = jnp.where(prow == pcol, 1.0, jnp.where(prow // 2 == pcol // 2, -packed, 0.0))
    block_mask = masks_ref[levels]
    for level in range(levels):
        inv_bf = inv.astype(BF16)
        inv_full = jnp.concatenate([inv_bf] * PACK, axis=0) * block_mask
        left = dot(inv_bf, lower * masks_ref[level])
        inv = inv - dot(left.astype(BF16), inv_full)
    inv_bf = inv.astype(BF16)
    inv_full = jnp.concatenate([inv_bf] * PACK, axis=0) * block_mask
    keys_f = keys.astype(F32)
    right = jnp.concatenate(
        [(-(pull_col * keys_f)).astype(BF16), (beta_col * values).astype(BF16)], axis=1
    )
    fresh = dot(inv_full, right).astype(BF16)
    outward = (keys_f * out_col).astype(BF16)
    result = []
    for p in range(PACK):
        block = slice(p * BLOCK, (p + 1) * BLOCK)
        carry = rows[4:5, p * BLOCK : p * BLOCK + 1]
        result.append((carry, contract(outward[block], fresh[block], 0, 0)))
    return result


def join(earlier, later):
    early_carry, early = earlier
    late_carry, late = later
    size = early.shape[0]
    grown = dot(late[:, :size].astype(BF16), early.astype(BF16))
    rest = jnp.concatenate([early_carry * late[:, :size], late[:, size:]], axis=1)
    return (early_carry * late_carry, late_carry * early + grown + rest)


def segment_kernel(
    seqs, dim, tok_ref, wk_ref, wv_ref, wgd_ref, shift_ref, rate_ref, extra_ref,
    out_ref, rows_ref, cols_ref, masks_ref, key_ref, value_ref,
):
    step = pl.program_id(0)

    @pl.when(step == 0)
    def _():
        prepare(tok_ref, wgd_ref, shift_ref, rate_ref, extra_ref, rows_ref, cols_ref, masks_ref)

    length = tok_ref.shape[0] // seqs
    per_step = wk_ref.shape[1] // dim
    span = PACK * BLOCK
    key_ref[...] = dot(tok_ref[...], wk_ref[...])
    value_ref[...] = dot(tok_ref[...], wv_ref[...])
    eye = lax.broadcasted_iota(jnp.int32, (dim, dim), 0) == lax.broadcasted_iota(
        jnp.int32, (dim, dim), 1
    )
    for j in range(per_step):
        head = step * per_step + j
        for s in range(seqs):
            terms = []
            for at in range(length // span):
                lanes = slice(s * length + at * span, s * length + (at + 1) * span)
                heads = slice(j * dim, (j + 1) * dim)
                key = key_ref[lanes, heads]
                key = key / (1.0 + jnp.exp(-key))
                key = key * lax.rsqrt(jnp.sum(key * key, axis=-1, keepdims=True) + EPS)
                value = value_ref[lanes, heads]
                value = (value / (1.0 + jnp.exp(-value))).astype(BF16).astype(F32)
                terms += pack_terms(
                    key.astype(BF16), value, rows_ref[head, :, lanes],
                    cols_ref[head, lanes, :], masks_ref,
                )
            while len(terms) > 1:
                terms = [join(terms[i], terms[i + 1]) for i in range(0, len(terms), 2)]
            carry, both = terms[0]
            diagonal = jnp.where(eye, carry, 0.0)
            out_ref[j * seqs + s, :, :dim] = both[:, :dim] + diagonal
            out_ref[j * seqs + s, :, dim:] = both[:, dim:]


def segment_maps(flat, key_matrix, value_matrix, wgd, shift, rate, extra, seqs, heads, dim):
    rows, width = flat.shape
    per_step = 2 if heads % 2 == 0 else 1
    span = PACK * BLOCK
    levels = BLOCK.bit_length() - 2
    whole = lambda shape: pl.BlockSpec(shape, lambda g: (0,) * len(shape))
    return pl.pallas_call(
        functools.partial(segment_kernel, seqs, dim),
        grid=(heads // per_step,),
        in_specs=[
            whole((rows, width)),
            pl.BlockSpec((width, per_step * dim), lambda g: (0, g)),
            pl.BlockSpec((width, per_step * dim), lambda g: (0, g)),
            whole(wgd.shape),
            whole(shift.shape),
            whole(rate.shape),
            whole(extra.shape),
        ],
        out_specs=pl.BlockSpec((per_step * seqs, dim, 2 * dim), lambda g: (g, 0, 0)),
        out_shape=jax.ShapeDtypeStruct((heads * seqs, dim, 2 * dim), F32),
        scratch_shapes=[
            pltpu.VMEM((heads, 8, rows), F32),
            pltpu.VMEM((heads, rows, 8), F32),
            pltpu.VMEM((levels + 1, span, span), BF16),
            pltpu.VMEM((rows, per_step * dim), F32),
            pltpu.VMEM((rows, per_step * dim), F32),
        ],
        compiler_params=pltpu.CompilerParams(
            dimension_semantics=("arbitrary",), vmem_limit_bytes=60 * 1024 * 1024
        ),
    )(flat, key_matrix, value_matrix, wgd, shift, rate, extra)


def token_step(final, info, gain):
    query, key, value, gate = (info[i : i + 1] for i in range(4))
    query = query * lax.rsqrt(jnp.sum(query * query, axis=-1, keepdims=True) + EPS)
    key = key * lax.rsqrt(jnp.sum(key * key, axis=-1, keepdims=True) + EPS)
    beta = 1.0 / (1.0 + jnp.exp(-gate))
    columns = jnp.transpose(jnp.concatenate([key, query, key * beta, key] + [key] * 4, axis=0))
    key_read = jnp.sum(columns[:, 0:1] * final, axis=0, keepdims=True)
    query_read = jnp.sum(columns[:, 1:2] * final, axis=0, keepdims=True)
    missing = value - key_read
    updated = final + columns[:, 2:3] * missing
    cross = jnp.sum(key * query, axis=-1, keepdims=True)
    read = (query_read + beta * cross * missing) / math.sqrt(final.shape[-1])
    read = read * lax.rsqrt(jnp.mean(read * read, axis=-1, keepdims=True) + EPS) * gain
    return updated, read


def first_pair(place, count, devices):
    start = 0
    bit = 1
    left = count
    while bit < devices:
        left //= 2
        start = start + lax.rem(place // bit, 2) * left if not isinstance(place, int) else (
            start + (place // bit) % 2 * left
        )
        bit *= 2
    return start


def exchange_kernel(
    devices, seqs, ab_ref, info_ref, gain_ref, state_ref, read_ref,
    got_ref, made_ref, out_buf, in_buf, read_buf, send_sem, recv_sem, put_sem, get_sem,
):
    me = lax.axis_index("sp")
    count, dim = ab_ref.shape[0], ab_ref.shape[1]
    barrier = pltpu.get_barrier_semaphore()
    for k in range(1, devices):
        pl.semaphore_signal(
            barrier, inc=1, device_id={"sp": lax.rem(me + k, devices)},
            device_id_type=pl.DeviceIdType.MESH,
        )
    pl.semaphore_wait(barrier, devices - 1)

    levels = devices.bit_length() - 1

    def halves(level):
        size = count >> (level + 1)
        bit = lax.rem(me // (1 << level), 2)
        return size, bit, bit * size, (1 - bit) * size

    def source(level, at):
        if level == 0:
            return ab_ref.at[at]
        return made_ref.at[made_base(level) + at]

    def made_base(level):
        return sum(count >> i for i in range(1, level))

    def copy(level, i):
        size, bit, keep, give = halves(level)
        slot = made_base(level + 1) + i
        partner = me + (1 - 2 * bit) * (1 << level)
        return pltpu.make_async_remote_copy(
            src_ref=source(level, give + i), dst_ref=got_ref.at[slot],
            send_sem=send_sem.at[slot], recv_sem=recv_sem.at[slot],
            device_id={"sp": partner}, device_id_type=pl.DeviceIdType.MESH,
        )

    for i in range(count // 2):
        copy(0, i).start()
    for level in range(levels):
        size, bit, keep, give = halves(level)
        base = made_base(level + 1)
        last = level == levels - 1
        if not last:
            nsize, nbit, nkeep, ngive = halves(level + 1)
        for i in range(size):
            if last:
                at = i
            elif i < nsize:
                at = ngive + i
            else:
                at = nkeep + (i - nsize)
            size_, bit_, keep_, give_ = size, bit, keep, give
            slot = base + at
            pltpu.make_async_remote_copy(
                src_ref=source(level, give + at), dst_ref=got_ref.at[slot],
                send_sem=send_sem.at[slot], recv_sem=recv_sem.at[slot],
                device_id={"sp": me + (1 - 2 * bit) * (1 << level)},
                device_id_type=pl.DeviceIdType.MESH,
            ).wait()
            mine = source(level, keep + at)[...]
            theirs = got_ref[slot]
            is_late = bit == 1
            late = jnp.where(is_late, mine, theirs)
            early = jnp.where(is_late, theirs, mine)
            late_map, late_add = late[:, :dim], late[:, dim:]
            if last:
                final = dot3(late_map, early[:, dim:]) + late_add
                pair = first_pair(me, count, devices) + i
                updated, read = token_step(final, info_ref[pair], gain_ref[...])
                out_buf[:, i, : dim // devices, :] = updated.reshape(devices, dim // devices, dim)
                out_buf[:, i, dim // devices :, :] = jnp.broadcast_to(read, (devices, 8, dim))
            else:
                grown = dot3(late_map, early)
                made_ref[slot, :, :dim] = grown[:, :dim]
                made_ref[slot, :, dim:] = grown[:, dim:] + late_add
                if i < nsize:
                    copy(level + 1, i).start()

    def put(k):
        dest = lax.rem(me + k, devices)
        return pltpu.make_async_remote_copy(
            src_ref=out_buf.at[dest], dst_ref=in_buf.at[me],
            send_sem=put_sem.at[k], recv_sem=get_sem.at[k],
            device_id={"sp": dest}, device_id_type=pl.DeviceIdType.MESH,
        )

    for k in range(1, devices):
        put(k).start()
    in_buf[me] = out_buf[me]
    for k in range(1, devices):
        put(k).wait()
    own = count // devices
    rows = dim // devices
    for e in range(devices):
        for i in range(own):
            pair = first_pair(e, count, devices) + i
            h, s = pair // seqs, pair % seqs
            state_ref[s, h] = in_buf[e, i, :rows, :].astype(BF16)
            read_buf[s, h : h + 1, :] = in_buf[e, i, rows : rows + 1, :]
    read_ref[...] = read_buf[...].astype(BF16)


def exchange(ab, info, gain, seqs, heads, devices):
    count, dim = ab.shape[0], ab.shape[1]
    slots = count - count // devices
    vmem = pl.BlockSpec(memory_space=pltpu.VMEM)
    return pl.pallas_call(
        functools.partial(exchange_kernel, devices, seqs),
        in_specs=[vmem] * 3,
        out_specs=[vmem] * 2,
        out_shape=[
            jax.ShapeDtypeStruct((seqs, heads, dim // devices, dim), BF16),
            jax.ShapeDtypeStruct((seqs, heads, dim), BF16),
        ],
        scratch_shapes=[
            pltpu.VMEM((slots, dim, 2 * dim), F32),
            pltpu.VMEM((slots, dim, 2 * dim), F32),
            pltpu.VMEM((devices, count // devices, dim // devices + 8, dim), F32),
            pltpu.VMEM((devices, count // devices, dim // devices + 8, dim), F32),
            pltpu.VMEM((seqs, heads, dim), F32),
            pltpu.SemaphoreType.DMA((slots,)),
            pltpu.SemaphoreType.DMA((slots,)),
            pltpu.SemaphoreType.DMA((devices,)),
            pltpu.SemaphoreType.DMA((devices,)),
        ],
        compiler_params=pltpu.CompilerParams(
            collective_id=0, has_side_effects=True, vmem_limit_bytes=40 * 1024 * 1024
        ),
    )(ab, info, gain)


def gathered_exchange(ab, info, gain, seqs, heads, devices):
    count, dim = ab.shape[0], ab.shape[1]
    everyone = lax.all_gather(ab, "sp")

    def one(at, state):
        step = lax.dynamic_index_in_dim(everyone, at, 0, False)
        return (
            jnp.matmul(step[..., :dim], state, precision=lax.Precision.HIGHEST) + step[..., dim:]
        )

    final = lax.fori_loop(0, devices, one, jnp.zeros((count, dim, dim), F32))
    updated, read = jax.vmap(lambda f, i: token_step(f, i, gain))(final, info)
    rows = dim // devices
    mine = lax.dynamic_slice_in_dim(updated, lax.axis_index("sp") * rows, rows, 1)
    mine = jnp.swapaxes(mine.reshape(heads, seqs, rows, dim), 0, 1)
    return mine.astype(BF16), jnp.swapaxes(read.reshape(heads, seqs, dim), 0, 1).astype(BF16)


def shards(
    tokens, key_matrix, value_matrix, gate_matrix, decay_matrix, gate_bias_offset,
    head_log_decay_rate, extra_log_decay, next_token_query, next_token_key,
    next_token_value, next_token_gate, readout_norm_gain,
):
    seqs, length, width = tokens.shape
    dim = next_token_key.shape[-1]
    heads = key_matrix.shape[1] // dim
    devices = lax.axis_size("sp")
    first = lax.axis_index("tp") * heads
    flat = tokens.reshape(seqs * length, width)
    pick = lambda array, axis: lax.dynamic_slice_in_dim(array, first, heads, axis)
    wgd = jnp.concatenate([pick(gate_matrix, 1), pick(decay_matrix, 1)], axis=1).T
    shift = pick(gate_bias_offset, 0)[:, None]
    rate = pick(head_log_decay_rate, 0)[:, None]
    extra = extra_log_decay.reshape(seqs * length, heads).T
    ab = segment_maps(
        flat, key_matrix, value_matrix, wgd, shift, rate, extra, seqs, heads, dim
    )
    wide = lambda array: jnp.swapaxes(array.astype(F32), 0, 1).reshape(heads * seqs, 1, dim)
    gate = jnp.broadcast_to(next_token_gate[..., None], next_token_key.shape)
    info = jnp.concatenate(
        [wide(next_token_query), wide(next_token_key), wide(next_token_value), wide(gate)], axis=1
    )
    gain = readout_norm_gain[None, :]
    whole = (seqs * heads) % devices == 0 and devices & (devices - 1) == 0 and devices > 1
    run = exchange if whole else gathered_exchange
    return run(ab, info, gain, seqs, heads, devices)


def solution(mesh):
    return jax.shard_map(
        shards,
        mesh=mesh,
        in_specs=(
            P("gr", "sp", None), P(None, "tp"), P(None, "tp"), P(), P(), P(), P(),
            P("gr", "sp", "tp"), P("gr", "tp", None), P("gr", "tp", None),
            P("gr", "tp", None), P("gr", "tp"), P(),
        ),
        out_specs=(P("gr", "tp", "sp", None), P("gr", "tp", None)),
        check_vma=False,
    )
```

profile of v0, /device:TPU:0, one launch (start us, length us, event | category | flops | bytes accessed | tf_op | source)
XLA Modules:
  0.0 133.1 jit_solution(12840584874660970035)
XLA Ops:
  0.6 0.8 constant_dynamic-slice_fusion
  1.4 0.6 maximum_bitcast_fusion.wgd_ref
  2.1 0.7 dynamic-slice_bitcast_fusion
  2.8 0.7 copy.15.shift_ref
  3.5 0.7 copy.16.rate_ref
  4.1 0.0 copy-start.2
  4.2 0.0 copy-start.3
  4.2 0.0 copy-start.4
  4.2 0.0 copy-start.5
  4.2 0.0 copy-start.1
  4.2 73.3 %shard_map.140.ab_ref = f32[16,128,256]{2,1,0:T(8,128)} custom-call(bf16[1024,2048]{1,0:T(8,128)(2,1)} %bitcast.24, bf16[2048,1024]{1,0:T(8,128)(2,1)} %wk_ref.1, bf16[2048,1024]{1,0:T(8,128)(2,1)} %wv_ref.1, bf16[16,2048]{1,0:T(8,128)(2,1)} %maximum_bitcast_fusion.wgd_ref, f32[8,1]{1,0:T(8,128)} %copy.15.shift_ref, f32[8,1]{1,0:T(8,128)} %copy.16.rate_ref, ...), custom_call_target="tpu_custom_call" | custom-call | tf_op jit(solution)/shard_map/pallas_call | solution.py:192
  77.5 0.0 copy-done.2
  77.5 0.0 copy-done.3
  77.6 0.0 copy-done.4
  77.6 0.0 copy-done.5
  77.6 0.1 copy.20
  77.7 0.1 broadcast_in_dim.17
  77.8 0.0 copy-done.1
  77.8 0.0 copy-start
  77.8 1.6 %copy-done = f32[16,128,256]{2,1,0:T(8,128)S(1)} copy-done((f32[16,128,256]{2,1,0:T(8,128)S(1)}, f32[16,128,256]{2,1,0:T(8,128)}, u32[]{:S(2)}) %copy-start) | copy-done | bytes 2097176
  79.4 52.5 %shard_map.141 = (bf16[2,8,16,128]{3,2,1,0:T(8,128)(2,1)S(1)}, bf16[2,8,128]{2,1,0:T(8,128)(2,1)S(1)}) custom-call(f32[16,128,256]{2,1,0:T(8,128)S(1)} %copy-done, f32[16,4,128]{2,1,0:T(4,128)S(1)} %pad_maximum_fusion.info_ref, f32[1,128]{1,0:T(1,128)S(1)} %bitcast.23), custom_call_target="tpu_custom_call" | custom-call | tf_op jit(solution)/shard_map/pallas_call | solution.py:357
  131.9 0.6 copy.23
  132.5 0.6 copy.24
  (7 shorter events, 0.1 us)
Async XLA Ops:
  4.1 73.4 %copy-start.2 = (bf16[2,8,128]{2,1,0:T(8,128)(2,1)S(1)}, bf16[2,8,128]{2,1,0:T(8,128)(2,1)}, u32[]{:S(2)}) copy-start(bf16[2,8,128]{2,1,0:T(8,128)(2,1)} %param.23) | copy-start | bytes 12292
  4.2 73.4 %copy-start.3 = (bf16[2,8,128]{2,1,0:T(8,128)(2,1)S(1)}, bf16[2,8,128]{2,1,0:T(8,128)(2,1)}, u32[]{:S(2)}) copy-start(bf16[2,8,128]{2,1,0:T(8,128)(2,1)} %param.21) | copy-start | bytes 12292
  4.2 73.4 %copy-start.4 = (bf16[2,8,128]{2,1,0:T(8,128)(2,1)S(1)}, bf16[2,8,128]{2,1,0:T(8,128)(2,1)}, u32[]{:S(2)}) copy-start(bf16[2,8,128]{2,1,0:T(8,128)(2,1)} %param.22) | copy-start | bytes 12292
  4.2 73.4 %copy-start.5 = (f32[2,8]{1,0:T(2,128)S(1)}, f32[2,8]{1,0:T(2,128)}, u32[]{:S(2)}) copy-start(f32[2,8]{1,0:T(2,128)} %param.24) | copy-start | bytes 196
  4.2 73.6 %copy-start.1 = (f32[128]{0:T(128)S(1)}, f32[128]{0:T(128)}, u32[]{:S(2)}) copy-start(f32[128]{0:T(128)} %param.25) | copy-start | bytes 1540
  77.8 1.6 %copy-start = (f32[16,128,256]{2,1,0:T(8,128)S(1)}, f32[16,128,256]{2,1,0:T(8,128)}, u32[]{:S(2)}) copy-start(f32[16,128,256]{2,1,0:T(8,128)} %shard_map.140.ab_ref) | copy-start | bytes 6291460
where the time goes:
time: 133 us
  Pallas kernels  126 us (95%)
  local copies, waits for them, and re-layouts  5.88 us (4%)
    pallas_call x1, Pallas kernels, segment_maps(): pl.pallas_call(functools.partial(segment_kernel, seqs, dim), grid=(heads...  73.3 us
    pallas_call x1, Pallas kernels, exchange(): pl.pallas_call(functools.partial(exchange_kernel, devices, seqs), in_spec...  52.5 us
    unnamed x15, local copies, waits for them, and re-layouts  2.91 us

commit v1 on v0

--- a/solution.py
+++ b/solution.py
@@ -92,43 +92,52 @@
             cols_ref[h, lanes, :] = jnp.transpose(stack)
 
 
-def pack_terms(keys, values, rows, cols, masks_ref):
+def pack_terms(packs, masks_ref):
     span = PACK * BLOCK
     levels = masks_ref.shape[0] - 1
     row = lax.broadcasted_iota(jnp.int32, (span, span), 0)
     col = lax.broadcasted_iota(jnp.int32, (span, span), 1)
     strict = (row // BLOCK == col // BLOCK) & (row > col)
-    cum_col, beta_col, pull_col, out_col = (cols[:, i : i + 1] for i in range(4))
-    cum_row = rows[0:1]
-    gram = contract(keys, keys, 1, 1)
-    scale = jnp.exp(jnp.where(strict, cum_col - cum_row, -1e30))
-    lower = (beta_col * gram) * scale
-    packed = lower[0:BLOCK]
-    for p in range(1, PACK):
-        packed = packed + lower[p * BLOCK : (p + 1) * BLOCK]
-    lower = lower.astype(BF16)
     prow = lax.broadcasted_iota(jnp.int32, (BLOCK, span), 0)
     pcol = lax.rem(lax.broadcasted_iota(jnp.int32, (BLOCK, span), 1), BLOCK)
-    inv = jnp.where(prow == pcol, 1.0, jnp.where(prow // 2 == pcol // 2, -packed, 0.0))
+    unit = prow == pcol
+    couple = prow // 2 == pcol // 2
+    lowers, invs, rights, outwards = [], [], [], []
+    for keys, values, rows, cols in packs:
+        cum_col, beta_col, pull_col, out_col = (cols[:, i : i + 1] for i in range(4))
+        gram = contract(keys, keys, 1, 1)
+        scale = jnp.exp(jnp.where(strict, cum_col - rows[0:1], -1e30))
+        lower = (beta_col * gram) * scale
+        packed = lower[0:BLOCK]
+        for p in range(1, PACK):
+            packed = packed + lower[p * BLOCK : (p + 1) * BLOCK]
+        lowers.append(lower.astype(BF16))
+        invs.append(jnp.where(unit, 1.0, jnp.where(couple, -packed, 0.0)))
+        keys_f = keys.astype(F32)
+        rights.append(
+            jnp.concatenate(
+                [(-(pull_col * keys_f)).astype(BF16), (beta_col * values).astype(BF16)], axis=1
+            )
+        )
+        outwards.append((keys_f * out_col).astype(BF16))
     block_mask = masks_ref[levels]
+    widen = lambda inv: jnp.concatenate([inv] * PACK, axis=0) * block_mask
     for level in range(levels):
-        inv_bf = inv.astype(BF16)
-        inv_full = jnp.concatenate([inv_bf] * PACK, axis=0) * block_mask
-        left = dot(inv_bf, lower * masks_ref[level])
-        inv = inv - dot(left.astype(BF16), inv_full)
-    inv_bf = inv.astype(BF16)
-    inv_full = jnp.concatenate([inv_bf] * PACK, axis=0) * block_mask
-    keys_f = keys.astype(F32)
-    right = jnp.concatenate(
-        [(-(pull_col * keys_f)).astype(BF16), (beta_col * values).astype(BF16)], axis=1
-    )
-    fresh = dot(inv_full, right).astype(BF16)
-    outward = (keys_f * out_col).astype(BF16)
+        mask = masks_ref[level]
+        narrow = [inv.astype(BF16) for inv in invs]
+        lefts = [dot(n, lower * mask).astype(BF16) for n, lower in zip(narrow, lowers)]
+        invs = [inv - dot(left, widen(n)) for inv, left, n in zip(invs, lefts, narrow)]
+    fresh = [
+        dot(widen(inv.astype(BF16)), right).astype(BF16) for inv, right in zip(invs, rights)
+    ]
     result = []
-    for p in range(PACK):
-        block = slice(p * BLOCK, (p + 1) * BLOCK)
-        carry = rows[4:5, p * BLOCK : p * BLOCK + 1]
-        result.append((carry, contract(outward[block], fresh[block], 0, 0)))
+    for (_, _, rows, _), outward, new in zip(packs, outwards, fresh):
+        terms = []
+        for p in range(PACK):
+            block = slice(p * BLOCK, (p + 1) * BLOCK)
+            carry = rows[4:5, p * BLOCK : p * BLOCK + 1]
+            terms.append((carry, contract(outward[block], new[block], 0, 0)))
+        result.append(terms)
     return result
 
 
@@ -141,8 +150,13 @@
     return (early_carry * late_carry, late_carry * early + grown + rest)
 
 
+def silu(array):
+    half = 0.5 * array
+    return half + half * jnp.tanh(half)
+
+
 def segment_kernel(
-    seqs, dim, tok_ref, wk_ref, wv_ref, wgd_ref, shift_ref, rate_ref, extra_ref,
+    seqs, dim, first_ref, tok_ref, wk_ref, wv_ref, wgd_ref, shift_ref, rate_ref, extra_ref,
     out_ref, rows_ref, cols_ref, masks_ref, key_ref, value_ref,
 ):
     step = pl.program_id(0)
@@ -159,61 +173,72 @@
     eye = lax.broadcasted_iota(jnp.int32, (dim, dim), 0) == lax.broadcasted_iota(
         jnp.int32, (dim, dim), 1
     )
+    packs = []
     for j in range(per_step):
-        head = step * per_step + j
-        for s in range(seqs):
-            terms = []
-            for at in range(length // span):
-                lanes = slice(s * length + at * span, s * length + (at + 1) * span)
-                heads = slice(j * dim, (j + 1) * dim)
-                key = key_ref[lanes, heads]
-                key = key / (1.0 + jnp.exp(-key))
-                key = key * lax.rsqrt(jnp.sum(key * key, axis=-1, keepdims=True) + EPS)
-                value = value_ref[lanes, heads]
-                value = (value / (1.0 + jnp.exp(-value))).astype(BF16).astype(F32)
-                terms += pack_terms(
-                    key.astype(BF16), value, rows_ref[head, :, lanes],
-                    cols_ref[head, lanes, :], masks_ref,
-                )
-            while len(terms) > 1:
-                terms = [join(terms[i], terms[i + 1]) for i in range(0, len(terms), 2)]
-            carry, both = terms[0]
-            diagonal = jnp.where(eye, carry, 0.0)
-            out_ref[j * seqs + s, :, :dim] = both[:, :dim] + diagonal
-            out_ref[j * seqs + s, :, dim:] = both[:, dim:]
-
-
-def segment_maps(flat, key_matrix, value_matrix, wgd, shift, rate, extra, seqs, heads, dim):
+        head = (first_ref[0] + step) * per_step + j
+        heads = slice(j * dim, (j + 1) * dim)
+        for at in range(seqs * length // span):
+            lanes = slice(at * span, (at + 1) * span)
+            key = silu(key_ref[lanes, heads])
+            key = key * lax.rsqrt(jnp.sum(key * key, axis=-1, keepdims=True) + EPS)
+            value = silu(value_ref[lanes, heads]).astype(BF16).astype(F32)
+            packs.append(
+                (key.astype(BF16), value, rows_ref[head, :, lanes], cols_ref[head, lanes, :])
+            )
+    terms = pack_terms(packs, masks_ref)
+    each = length // span
+    chains = [
+        sum(terms[i * each : (i + 1) * each], []) for i in range(per_step * seqs)
+    ]
+    while len(chains[0]) > 1:
+        chains = [
+            [join(chain[i], chain[i + 1]) for i in range(0, len(chain), 2)] for chain in chains
+        ]
+    for i, chain in enumerate(chains):
+        carry, both = chain[0]
+        out_ref[i, :, :dim] = both[:, :dim] + jnp.where(eye, carry, 0.0)
+        out_ref[i, :, dim:] = both[:, dim:]
+
+
+def segment_maps(
+    first, some, flat, key_matrix, value_matrix, wgd, shift, rate, extra, seqs, heads, dim
+):
     rows, width = flat.shape
-    per_step = 2 if heads % 2 == 0 else 1
+    per_step = 2 if some % 2 == 0 else 1
     span = PACK * BLOCK
     levels = BLOCK.bit_length() - 2
-    whole = lambda shape: pl.BlockSpec(shape, lambda g: (0,) * len(shape))
+    whole = lambda shape: pl.BlockSpec(shape, lambda g, first: (0,) * len(shape))
+    weights = pl.BlockSpec((width, per_step * dim), lambda g, first: (0, first[0] + g))
+    steps = some // per_step
     return pl.pallas_call(
         functools.partial(segment_kernel, seqs, dim),
-        grid=(heads // per_step,),
-        in_specs=[
-            whole((rows, width)),
-            pl.BlockSpec((width, per_step * dim), lambda g: (0, g)),
-            pl.BlockSpec((width, per_step * dim), lambda g: (0, g)),
-            whole(wgd.shape),
-            whole(shift.shape),
-            whole(rate.shape),
-            whole(extra.shape),
-        ],
-        out_specs=pl.BlockSpec((per_step * seqs, dim, 2 * dim), lambda g: (g, 0, 0)),
-        out_shape=jax.ShapeDtypeStruct((heads * seqs, dim, 2 * dim), F32),
-        scratch_shapes=[
-            pltpu.VMEM((heads, 8, rows), F32),
-            pltpu.VMEM((heads, rows, 8), F32),
-            pltpu.VMEM((levels + 1, span, span), BF16),
-            pltpu.VMEM((rows, per_step * dim), F32),
-            pltpu.VMEM((rows, per_step * dim), F32),
-        ],
+        grid_spec=pltpu.PrefetchScalarGridSpec(
+            num_scalar_prefetch=1,
+            grid=(steps,),
+            in_specs=[
+                whole((rows, width)), weights, weights, whole(wgd.shape), whole(shift.shape),
+                whole(rate.shape), whole(extra.shape),
+            ],
+            out_specs=pl.BlockSpec(
+                (per_step * seqs, dim, 2 * dim), lambda g, first: (g, 0, 0)
+            ),
+            scratch_shapes=[
+                pltpu.VMEM((heads, 8, rows), F32),
+                pltpu.VMEM((heads, rows, 8), F32),
+                pltpu.VMEM((levels + 1, span, span), BF16),
+                pltpu.VMEM((rows, per_step * dim), F32),
+                pltpu.VMEM((rows, per_step * dim), F32),
+            ],
+        ),
+        out_shape=jax.ShapeDtypeStruct((some * seqs, dim, 2 * dim), F32),
         compiler_params=pltpu.CompilerParams(
-            dimension_semantics=("arbitrary",), vmem_limit_bytes=60 * 1024 * 1024
+            dimension_semantics=("arbitrary",), vmem_limit_bytes=48 * 1024 * 1024
         ),
-    )(flat, key_matrix, value_matrix, wgd, shift, rate, extra)
+        cost_estimate=pl.CostEstimate(
+            flops=8 * rows * width * some * dim, transcendentals=0,
+            bytes_accessed=2 * rows * width + 4 * width * some * dim,
+        ),
+    )(first * steps, flat, key_matrix, value_matrix, wgd, shift, rate, extra)
 
 
 def token_step(final, info, gain):
@@ -246,11 +271,11 @@
 
 
 def exchange_kernel(
-    devices, seqs, ab_ref, info_ref, gain_ref, state_ref, read_ref,
+    devices, seqs, ab_ref, other_ref, info_ref, gain_ref, state_ref, read_ref,
     got_ref, made_ref, out_buf, in_buf, read_buf, send_sem, recv_sem, put_sem, get_sem,
 ):
     me = lax.axis_index("sp")
-    count, dim = ab_ref.shape[0], ab_ref.shape[1]
+    count, dim = 2 * ab_ref.shape[0], ab_ref.shape[1]
     barrier = pltpu.get_barrier_semaphore()
     for k in range(1, devices):
         pl.semaphore_signal(
@@ -266,65 +291,60 @@
         bit = lax.rem(me // (1 << level), 2)
         return size, bit, bit * size, (1 - bit) * size
 
-    def source(level, at):
-        if level == 0:
-            return ab_ref.at[at]
-        return made_ref.at[made_base(level) + at]
-
     def made_base(level):
         return sum(count >> i for i in range(1, level))
 
-    def copy(level, i):
+    def mine_at(level, at):
+        if level == 0:
+            return ab_ref[at]
+        return made_ref[made_base(level) + halves(level)[2] + at]
+
+    def order(level):
+        size = count >> (level + 1)
+        if level == levels - 1:
+            return list(range(size))
+        _, _, keep, give = halves(level + 1)
+        after = order(level + 1)
+        return [give + i for i in after] + [keep + i for i in after]
+
+    def copy(level, at):
         size, bit, keep, give = halves(level)
-        slot = made_base(level + 1) + i
-        partner = me + (1 - 2 * bit) * (1 << level)
+        slot = made_base(level + 1) - count // 2 + at
         return pltpu.make_async_remote_copy(
-            src_ref=source(level, give + i), dst_ref=got_ref.at[slot],
+            src_ref=made_ref.at[made_base(level) + give + at], dst_ref=got_ref.at[slot],
             send_sem=send_sem.at[slot], recv_sem=recv_sem.at[slot],
-            device_id={"sp": partner}, device_id_type=pl.DeviceIdType.MESH,
-        )
-
-    for i in range(count // 2):
-        copy(0, i).start()
+            device_id={"sp": me + (1 - 2 * bit) * (1 << level)},
+            device_id_type=pl.DeviceIdType.MESH,
+        )
+
     for level in range(levels):
         size, bit, keep, give = halves(level)
-        base = made_base(level + 1)
         last = level == levels - 1
-        if not last:
-            nsize, nbit, nkeep, ngive = halves(level + 1)
-        for i in range(size):
-            if last:
-                at = i
-            elif i < nsize:
-                at = ngive + i
+        after = [] if last else order(level + 1)
+        for turn, at in enumerate(order(level)):
+            mine = mine_at(level, at)
+            if level == 0:
+                theirs = other_ref[at]
             else:
-                at = nkeep + (i - nsize)
-            size_, bit_, keep_, give_ = size, bit, keep, give
-            slot = base + at
-            pltpu.make_async_remote_copy(
-                src_ref=source(level, give + at), dst_ref=got_ref.at[slot],
-                send_sem=send_sem.at[slot], recv_sem=recv_sem.at[slot],
-                device_id={"sp": me + (1 - 2 * bit) * (1 << level)},
-                device_id_type=pl.DeviceIdType.MESH,
-            ).wait()
-            mine = source(level, keep + at)[...]
-            theirs = got_ref[slot]
+                copy(level, at).wait()
+                theirs = got_ref[made_base(level + 1) - count // 2 + at]
             is_late = bit == 1
             late = jnp.where(is_late, mine, theirs)
             early = jnp.where(is_late, theirs, mine)
             late_map, late_add = late[:, :dim], late[:, dim:]
             if last:
                 final = dot3(late_map, early[:, dim:]) + late_add
-                pair = first_pair(me, count, devices) + i
+                pair = first_pair(me, count, devices) + at
                 updated, read = token_step(final, info_ref[pair], gain_ref[...])
-                out_buf[:, i, : dim // devices, :] = updated.reshape(devices, dim // devices, dim)
-                out_buf[:, i, dim // devices :, :] = jnp.broadcast_to(read, (devices, 8, dim))
+                out_buf[:, at, : dim // devices, :] = updated.reshape(devices, dim // devices, dim)
+                out_buf[:, at, dim // devices :, :] = jnp.broadcast_to(read, (devices, 8, dim))
             else:
                 grown = dot3(late_map, early)
+                slot = made_base(level + 1) + at
                 made_ref[slot, :, :dim] = grown[:, :dim]
                 made_ref[slot, :, dim:] = grown[:, dim:] + late_add
-                if i < nsize:
-                    copy(level + 1, i).start()
+                if turn < len(after):
+                    copy(level + 1, after[turn]).start()
 
     def put(k):
         dest = lax.rem(me + k, devices)
@@ -350,13 +370,13 @@
     read_ref[...] = read_buf[...].astype(BF16)
 
 
-def exchange(ab, info, gain, seqs, heads, devices):
-    count, dim = ab.shape[0], ab.shape[1]
-    slots = count - count // devices
+def exchange(ab, other, info, gain, seqs, heads, devices):
+    count, dim = 2 * ab.shape[0], ab.shape[1]
+    slots = count // 2 - count // devices
     vmem = pl.BlockSpec(memory_space=pltpu.VMEM)
     return pl.pallas_call(
         functools.partial(exchange_kernel, devices, seqs),
-        in_specs=[vmem] * 3,
+        in_specs=[vmem] * 4,
         out_specs=[vmem] * 2,
         out_shape=[
             jax.ShapeDtypeStruct((seqs, heads, dim // devices, dim), BF16),
@@ -364,7 +384,7 @@
         ],
         scratch_shapes=[
             pltpu.VMEM((slots, dim, 2 * dim), F32),
-            pltpu.VMEM((slots, dim, 2 * dim), F32),
+            pltpu.VMEM((slots + count // devices + count // 2, dim, 2 * dim), F32),
             pltpu.VMEM((devices, count // devices, dim // devices + 8, dim), F32),
             pltpu.VMEM((devices, count // devices, dim // devices + 8, dim), F32),
             pltpu.VMEM((seqs, heads, dim), F32),
@@ -376,7 +396,7 @@
         compiler_params=pltpu.CompilerParams(
             collective_id=0, has_side_effects=True, vmem_limit_bytes=40 * 1024 * 1024
         ),
-    )(ab, info, gain)
+    )(ab, other, info, gain)
 
 
 def gathered_exchange(ab, info, gain, seqs, heads, devices):
@@ -413,18 +433,24 @@
     shift = pick(gate_bias_offset, 0)[:, None]
     rate = pick(head_log_decay_rate, 0)[:, None]
     extra = extra_log_decay.reshape(seqs * length, heads).T
-    ab = segment_maps(
-        flat, key_matrix, value_matrix, wgd, shift, rate, extra, seqs, heads, dim
-    )
     wide = lambda array: jnp.swapaxes(array.astype(F32), 0, 1).reshape(heads * seqs, 1, dim)
     gate = jnp.broadcast_to(next_token_gate[..., None], next_token_key.shape)
     info = jnp.concatenate(
         [wide(next_token_query), wide(next_token_key), wide(next_token_value), wide(gate)], axis=1
     )
     gain = readout_norm_gain[None, :]
-    whole = (seqs * heads) % devices == 0 and devices & (devices - 1) == 0 and devices > 1
-    run = exchange if whole else gathered_exchange
-    return run(ab, info, gain, seqs, heads, devices)
+    maps = lambda at, some: segment_maps(
+        jnp.full((1,), at, jnp.int32), some, flat, key_matrix, value_matrix, wgd, shift, rate,
+        extra, seqs, heads, dim,
+    )
+    paired = devices & (devices - 1) == 0 and devices > 2 and heads % 2 == 0
+    if not paired or (seqs * heads) % devices:
+        return gathered_exchange(maps(0, heads), info, gain, seqs, heads, devices)
+    late = lax.rem(lax.axis_index("sp"), 2)
+    given = maps(1 - late, heads // 2)
+    other = lax.ppermute(given, "sp", [(i, i ^ 1) for i in range(devices)])
+    kept = maps(late, heads // 2)
+    return exchange(kept, other, info, gain, seqs, heads, devices)
 
 
 def solution(mesh):

time: 133 us -> 81.1 us (0.61)
  Pallas kernels: 126 us -> 65.3 us
  waiting for transfers between devices: 0 us -> 3.34 us
  starting transfers between devices: 0 us -> 3.07 us
  local copies, waits for them, and re-layouts: 5.88 us -> 8.24 us
    pallas_call x1 -> x2, Pallas kernels: 73.3 us -> 34.6 us  [segment_maps(): pl.pallas_call(functools.partial(segment_kernel, seqs, dim), grid_spec=pl...]
    pallas_call x1, Pallas kernels: 52.5 us -> 30.7 us  [exchange(): pl.pallas_call(functools.partial(exchange_kernel, devices, seqs), in_spec...]
    unnamed x15 -> x21, local copies, waits for them, and re-layouts: 2.91 us -> 6.45 us
    ppermute x0 -> x1, waiting for transfers between devices: none -> 3.34 us  [shards(): other = lax.ppermute(given, 'sp', [(i, i ^ 1) for i in range(devices)])]
    ppermute x0 -> x1, starting transfers between devices: none -> 3.07 us  [shards(): other = lax.ppermute(given, 'sp', [(i, i ^ 1) for i in range(devices)])]
  transfers between devices with their start and end apart: 0 -> 1, of which waited for: 0 -> 1; matrix products, arithmetic and copies ran while one was open for 0% -> 0% of each run, Pallas kernels for 0% -> 21%
where the time goes in v1:
time: 81.1 us; the launch traced here: 80.8 us
  Pallas kernels  65.3 us (81%)
  local copies, waits for them, and re-layouts  8.24 us (10%)
  waiting for transfers between devices  3.34 us (4%)
  starting transfers between devices  3.07 us (4%)
    pallas_call x2, Pallas kernels, segment_maps(): pl.pallas_call(functools.partial(segment_kernel, seqs, dim), grid_spec=pl...  34.6 us
    pallas_call x1, Pallas kernels, exchange(): pl.pallas_call(functools.partial(exchange_kernel, devices, seqs), in_spec...  30.7 us
    unnamed x21, local copies, waits for them, and re-layouts  6.45 us
    ppermute x1, waiting for transfers between devices, shards(): other = lax.ppermute(given, 'sp', [(i, i ^ 1) for i in range(devices)])  3.34 us
    ppermute x1, starting transfers between devices, shards(): other = lax.ppermute(given, 'sp', [(i, i ^ 1) for i in range(devices)])  3.07 us
  transfers between devices with their start and end apart: 1, of which 1 were waited for; matrix products, arithmetic and copies ran while one was open for 0% of the time, Pallas kernels for 21%

profile of v1, /device:TPU:0, one launch (start us, length us, event | category | flops | bytes accessed | tf_op | source)
XLA Modules:
  0.0 80.8 jit_solution(6964302642952945827)
XLA Ops:
  0.6 0.8 dynamic-slice_bitcast_fusion
  1.4 0.1 copy.15.shift_ref
  1.5 0.1 copy.16.rate_ref
  1.6 0.8 constant_dynamic-slice_fusion
  2.3 0.0 copy-start.1
  2.4 2.2 %copy-done.1 = bf16[2,512,2048]{2,1,0:T(8,128)(2,1)S(1)} copy-done((bf16[2,512,2048]{2,1,0:T(8,128)(2,1)S(1)}, bf16[2,512,2048]{2,1,0:T(8,128)(2,1)}, u32[]{:S(2)}) %copy-start.1) | copy-done | bytes 4194328
  4.5 0.0 copy-start.3
  4.5 0.8 copy-done.3
  5.3 0.0 copy-start.5
  5.3 0.0 copy-start.6
  5.3 0.0 copy-start.7
  5.3 0.0 copy-start.8
  5.3 0.0 copy-start.4
  5.3 17.3 %shard_map.141 = f32[8,128,256]{2,1,0:T(8,128)S(1)} custom-call(s32[1]{0:T(128)} %bitcast.7.first_ref, bf16[1024,2048]{1,0:T(8,128)(2,1)S(1)} %bitcast.26, bf16[2048,1024]{1,0:T(8,128)(2,1)} %wk_ref.3, bf16[2048,1024]{1,0:T(8,128)(2,1)} %wv_ref.3, bf16[16,2048]{1,0:T(8,128)(2,1)S(1)} %maximum_bitcast_fusion.wgd_ref, f32[8,1]{1,0:T(8,128)S(1)} %copy.15.shift_ref, ...), custom_call_target="tpu_custom_call" | custom-call | flops 8589934592 | bytes 8388608 | tf_op jit(solution)/shard_map/pallas_call | solution.py:213
  22.7 3.1 %collective-permute-start = (f32[8,128,256]{2,1,0:T(8,128)S(1)}, f32[8,128,256]{2,1,0:T(8,128)S(1)}, u32[]{:S(2)}, u32[]{:S(2)}) collective-permute-start(f32[8,128,256]{2,1,0:T(8,128)S(1)} %shard_map.141), channel_id=1, source_target_pairs={{0,2},{2,0},{4,6},{6,4},{8,10},{10,8},{12,14},{14,12},{1,3},{3,1},... | collective-permute-start | bytes 3145736 | tf_op jit(solution)/shard_map/ppermute | solution.py:451
  25.7 0.0 copy-done.5
  25.7 0.0 copy-done.6
  25.8 0.0 copy-done.7
  25.8 0.0 copy-done.8
  25.8 0.1 copy.22
  25.9 0.1 broadcast_in_dim.19
  26.0 0.0 copy-done.4
  26.0 0.0 copy-start.2
  26.0 2.2 %copy-done.2 = bf16[2,512,2048]{2,1,0:T(8,128)(2,1)S(1)} copy-done((bf16[2,512,2048]{2,1,0:T(8,128)(2,1)S(1)}, bf16[2,512,2048]{2,1,0:T(8,128)(2,1)}, u32[]{:S(2)}) %copy-start.2) | copy-done | bytes 4194328
  28.2 0.0 copy-start
  28.2 17.3 %shard_map.140.ab_ref = f32[8,128,256]{2,1,0:T(8,128)S(1)} custom-call(s32[1]{0:T(128)} %bitcast.first_ref, bf16[1024,2048]{1,0:T(8,128)(2,1)S(1)} %bitcast.27, bf16[2048,1024]{1,0:T(8,128)(2,1)} %wk_ref.3, bf16[2048,1024]{1,0:T(8,128)(2,1)} %wv_ref.3, bf16[16,2048]{1,0:T(8,128)(2,1)S(1)} %maximum_bitcast_fusion.wgd_ref, f32[8,1]{1,0:T(8,128)S(1)} %copy.15.shift_ref, ...), custom_call_target="tpu_custom_call" | custom-call | flops 8589934592 | bytes 8388608 | tf_op jit(solution)/shard_map/pallas_call | solution.py:213
  45.5 3.3 %collective-permute-done.other_ref = f32[8,128,256]{2,1,0:T(8,128)S(1)} collective-permute-done((f32[8,128,256]{2,1,0:T(8,128)S(1)}, f32[8,128,256]{2,1,0:T(8,128)S(1)}, u32[]{:S(2)}, u32[]{:S(2)}) %collective-permute-start) | collective-permute-done | bytes 1048608 | tf_op jit(solution)/shard_map/ppermute | solution.py:451
  48.9 0.0 copy-done
  48.9 30.7 %shard_map.142 = (bf16[2,8,16,128]{3,2,1,0:T(8,128)(2,1)S(1)}, bf16[2,8,128]{2,1,0:T(8,128)(2,1)S(1)}) custom-call(f32[8,128,256]{2,1,0:T(8,128)S(1)} %shard_map.140.ab_ref, f32[8,128,256]{2,1,0:T(8,128)S(1)} %collective-permute-done.other_ref, f32[16,4,128]{2,1,0:T(4,128)S(1)} %pad_maximum_fusion.info_ref, f32[1,128]{1,0:T(1,128)S(1)} %bitcast.25), custom_call_target="tpu_custom_call" | custom-call | tf_op jit(solution)/shard_map/pallas_call | solution.py:377
  79.6 0.6 copy.25
  80.2 0.6 copy.26
  (8 shorter events, 0.1 us)
Async XLA Ops:
  2.3 2.2 %copy-start.1 = (bf16[2,512,2048]{2,1,0:T(8,128)(2,1)S(1)}, bf16[2,512,2048]{2,1,0:T(8,128)(2,1)}, u32[]{:S(2)}) copy-start(bf16[2,512,2048]{2,1,0:T(8,128)(2,1)} %param.13) | copy-start | bytes 12582916
  4.5 0.8 copy-start.3
  5.3 20.4 %copy-start.5 = (bf16[2,8,128]{2,1,0:T(8,128)(2,1)S(1)}, bf16[2,8,128]{2,1,0:T(8,128)(2,1)}, u32[]{:S(2)}) copy-start(bf16[2,8,128]{2,1,0:T(8,128)(2,1)} %param.21) | copy-start | bytes 12292
  5.3 20.4 %copy-start.6 = (bf16[2,8,128]{2,1,0:T(8,128)(2,1)S(1)}, bf16[2,8,128]{2,1,0:T(8,128)(2,1)}, u32[]{:S(2)}) copy-start(bf16[2,8,128]{2,1,0:T(8,128)(2,1)} %param.22) | copy-start | bytes 12292
  5.3 20.5 %copy-start.7 = (bf16[2,8,128]{2,1,0:T(8,128)(2,1)S(1)}, bf16[2,8,128]{2,1,0:T(8,128)(2,1)}, u32[]{:S(2)}) copy-start(bf16[2,8,128]{2,1,0:T(8,128)(2,1)} %param.23) | copy-start | bytes 12292
  5.3 20.5 %copy-start.8 = (f32[2,8]{1,0:T(2,128)S(1)}, f32[2,8]{1,0:T(2,128)}, u32[]{:S(2)}) copy-start(f32[2,8]{1,0:T(2,128)} %param.24) | copy-start | bytes 196
  5.3 20.7 %copy-start.4 = (f32[2,512,8]{1,2,0:T(8,128)S(1)}, f32[2,512,8]{1,2,0:T(8,128)}, u32[]{:S(2)}) copy-start(f32[2,512,8]{1,2,0:T(8,128)} %param.20) | copy-start | bytes 98308
  22.7 26.2 %collective-permute-start = (f32[8,128,256]{2,1,0:T(8,128)S(1)}, f32[8,128,256]{2,1,0:T(8,128)S(1)}, u32[]{:S(2)}, u32[]{:S(2)}) collective-permute-start(f32[8,128,256]{2,1,0:T(8,128)S(1)} %shard_map.141), channel_id=1, source_target_pairs={{0,2},{2,0},{4,6},{6,4},{8,10},{10,8},{12,14},{14,12},{1,3},{3,1},... | collective-permute-start | bytes 3145736 | tf_op jit(solution)/shard_map/ppermute | solution.py:451
  26.0 2.2 %copy-start.2 = (bf16[2,512,2048]{2,1,0:T(8,128)(2,1)S(1)}, bf16[2,512,2048]{2,1,0:T(8,128)(2,1)}, u32[]{:S(2)}) copy-start(bf16[2,512,2048]{2,1,0:T(8,128)(2,1)} %param.13) | copy-start | bytes 12582916
  28.2 20.7 %copy-start = (f32[128]{0:T(128)S(1)}, f32[128]{0:T(128)}, u32[]{:S(2)}) copy-start(f32[128]{0:T(128)} %param.25) | copy-start | bytes 1540

commit v2 on v1

--- a/solution.py
+++ b/solution.py
@@ -232,7 +232,7 @@
         ),
         out_shape=jax.ShapeDtypeStruct((some * seqs, dim, 2 * dim), F32),
         compiler_params=pltpu.CompilerParams(
-            dimension_semantics=("arbitrary",), vmem_limit_bytes=48 * 1024 * 1024
+            dimension_semantics=("arbitrary",), vmem_limit_bytes=56 * 1024 * 1024
         ),
         cost_estimate=pl.CostEstimate(
             flops=8 * rows * width * some * dim, transcendentals=0,
@@ -270,12 +270,40 @@
     return start
 
 
+def merge(is_late, mine, theirs):
+    dim = mine.shape[0]
+    late = jnp.where(is_late, mine, theirs)
+    early = jnp.where(is_late, theirs, mine)
+    grown = dot3(late[:, :dim], early)
+    return jnp.concatenate([grown[:, :dim], grown[:, dim:] + late[:, dim:]], axis=1)
+
+
+def merge_kernel(late_ref, mine_ref, theirs_ref, out_ref):
+    for i in range(mine_ref.shape[0]):
+        out_ref[i] = merge(late_ref[0] == 1, mine_ref[i], theirs_ref[i])
+
+
+def merge_pairs(late, mine, theirs):
+    vmem = pl.BlockSpec(memory_space=pltpu.VMEM)
+    count, dim, _ = mine.shape
+    return pl.pallas_call(
+        merge_kernel,
+        in_specs=[pl.BlockSpec(memory_space=pltpu.SMEM), vmem, vmem],
+        out_specs=vmem,
+        out_shape=jax.ShapeDtypeStruct(mine.shape, F32),
+        compiler_params=pltpu.CompilerParams(vmem_limit_bytes=16 * 1024 * 1024),
+        cost_estimate=pl.CostEstimate(
+            flops=12 * count * dim * dim * dim, transcendentals=0, bytes_accessed=12 * mine.size
+        ),
+    )(jnp.full((1,), late, jnp.int32), mine, theirs)
+
+
 def exchange_kernel(
-    devices, seqs, ab_ref, other_ref, info_ref, gain_ref, state_ref, read_ref,
+    devices, seqs, ab_ref, other_ref, next_ref, info_ref, gain_ref, state_ref, read_ref,
     got_ref, made_ref, out_buf, in_buf, read_buf, send_sem, recv_sem, put_sem, get_sem,
 ):
     me = lax.axis_index("sp")
-    count, dim = 2 * ab_ref.shape[0], ab_ref.shape[1]
+    count, dim = 4 * ab_ref.shape[0], ab_ref.shape[1]
     barrier = pltpu.get_barrier_semaphore()
     for k in range(1, devices):
         pl.semaphore_signal(
@@ -292,12 +320,10 @@
         return size, bit, bit * size, (1 - bit) * size
 
     def made_base(level):
-        return sum(count >> i for i in range(1, level))
-
-    def mine_at(level, at):
-        if level == 0:
-            return ab_ref[at]
-        return made_ref[made_base(level) + halves(level)[2] + at]
+        return sum(count >> i for i in range(2, level))
+
+    def got_base(level):
+        return sum(count >> i for i in range(3, level + 1))
 
     def order(level):
         size = count >> (level + 1)
@@ -309,7 +335,7 @@
 
     def copy(level, at):
         size, bit, keep, give = halves(level)
-        slot = made_base(level + 1) - count // 2 + at
+        slot = got_base(level) + at
         return pltpu.make_async_remote_copy(
             src_ref=made_ref.at[made_base(level) + give + at], dst_ref=got_ref.at[slot],
             send_sem=send_sem.at[slot], recv_sem=recv_sem.at[slot],
@@ -317,32 +343,29 @@
             device_id_type=pl.DeviceIdType.MESH,
         )
 
-    for level in range(levels):
+    for level in range(1, levels):
         size, bit, keep, give = halves(level)
         last = level == levels - 1
         after = [] if last else order(level + 1)
         for turn, at in enumerate(order(level)):
-            mine = mine_at(level, at)
-            if level == 0:
-                theirs = other_ref[at]
+            if level == 1:
+                mine = merge(halves(0)[1] == 1, ab_ref[at], other_ref[at])
+                theirs = next_ref[at]
             else:
                 copy(level, at).wait()
-                theirs = got_ref[made_base(level + 1) - count // 2 + at]
-            is_late = bit == 1
-            late = jnp.where(is_late, mine, theirs)
-            early = jnp.where(is_late, theirs, mine)
-            late_map, late_add = late[:, :dim], late[:, dim:]
+                mine = made_ref[made_base(level) + keep + at]
+                theirs = got_ref[got_base(level) + at]
             if last:
-                final = dot3(late_map, early[:, dim:]) + late_add
+                is_late = bit == 1
+                late = jnp.where(is_late, mine, theirs)
+                early = jnp.where(is_late, theirs, mine)
+                final = dot3(late[:, :dim], early[:, dim:]) + late[:, dim:]
                 pair = first_pair(me, count, devices) + at
                 updated, read = token_step(final, info_ref[pair], gain_ref[...])
                 out_buf[:, at, : dim // devices, :] = updated.reshape(devices, dim // devices, dim)
                 out_buf[:, at, dim // devices :, :] = jnp.broadcast_to(read, (devices, 8, dim))
             else:
-                grown = dot3(late_map, early)
-                slot = made_base(level + 1) + at
-                made_ref[slot, :, :dim] = grown[:, :dim]
-                made_ref[slot, :, dim:] = grown[:, dim:] + late_add
+                made_ref[made_base(level + 1) + at] = merge(bit == 1, mine, theirs)
                 if turn < len(after):
                     copy(level + 1, after[turn]).start()
 
@@ -370,13 +393,13 @@
     read_ref[...] = read_buf[...].astype(BF16)
 
 
-def exchange(ab, other, info, gain, seqs, heads, devices):
-    count, dim = 2 * ab.shape[0], ab.shape[1]
-    slots = count // 2 - count // devices
+def exchange(ab, other, following, info, gain, seqs, heads, devices):
+    count, dim = 4 * ab.shape[0], ab.shape[1]
+    slots = count // 4 - count // devices
     vmem = pl.BlockSpec(memory_space=pltpu.VMEM)
     return pl.pallas_call(
         functools.partial(exchange_kernel, devices, seqs),
-        in_specs=[vmem] * 4,
+        in_specs=[vmem] * 5,
         out_specs=[vmem] * 2,
         out_shape=[
             jax.ShapeDtypeStruct((seqs, heads, dim // devices, dim), BF16),
@@ -384,7 +407,7 @@
         ],
         scratch_shapes=[
             pltpu.VMEM((slots, dim, 2 * dim), F32),
-            pltpu.VMEM((slots + count // devices + count // 2, dim, 2 * dim), F32),
+            pltpu.VMEM((slots + count // devices + count // 4, dim, 2 * dim), F32),
             pltpu.VMEM((devices, count // devices, dim // devices + 8, dim), F32),
             pltpu.VMEM((devices, count // devices, dim // devices + 8, dim), F32),
             pltpu.VMEM((seqs, heads, dim), F32),
@@ -394,9 +417,9 @@
             pltpu.SemaphoreType.DMA((devices,)),
         ],
         compiler_params=pltpu.CompilerParams(
-            collective_id=0, has_side_effects=True, vmem_limit_bytes=40 * 1024 * 1024
-        ),
-    )(ab, other, info, gain)
+            collective_id=0, has_side_effects=True, vmem_limit_bytes=16 * 1024 * 1024
+        ),
+    )(ab, other, following, info, gain)
 
 
 def gathered_exchange(ab, info, gain, seqs, heads, devices):
@@ -439,18 +462,24 @@
         [wide(next_token_query), wide(next_token_key), wide(next_token_value), wide(gate)], axis=1
     )
     gain = readout_norm_gain[None, :]
-    maps = lambda at, some: segment_maps(
+    maps = lambda at, some, flat=flat: segment_maps(
         jnp.full((1,), at, jnp.int32), some, flat, key_matrix, value_matrix, wgd, shift, rate,
         extra, seqs, heads, dim,
     )
-    paired = devices & (devices - 1) == 0 and devices > 2 and heads % 2 == 0
+    paired = devices & (devices - 1) == 0 and devices > 4 and heads % 4 == 0
     if not paired or (seqs * heads) % devices:
         return gathered_exchange(maps(0, heads), info, gain, seqs, heads, devices)
-    late = lax.rem(lax.axis_index("sp"), 2)
-    given = maps(1 - late, heads // 2)
-    other = lax.ppermute(given, "sp", [(i, i ^ 1) for i in range(devices)])
-    kept = maps(late, heads // 2)
-    return exchange(kept, other, info, gain, seqs, heads, devices)
+    place = lax.axis_index("sp")
+    late, later = lax.rem(place, 2), lax.rem(place // 2, 2)
+    swap = lambda array, step: lax.ppermute(array, "sp", [(i, i ^ step) for i in range(devices)])
+    quarter = heads // 4
+    other_first = swap(maps(2 * (1 - late) + 1 - later, quarter), 1)
+    other = swap(maps(2 * (1 - late) + later, quarter), 1)
+    merged = merge_pairs(late, maps(2 * late + 1 - later, quarter), other_first)
+    flat, merged = lax.optimization_barrier((flat, merged))
+    following = swap(merged, 2)
+    kept = maps(2 * late + later, quarter, flat)
+    return exchange(kept, other, following, info, gain, seqs, heads, devices)
 
 
 def solution(mesh):

time: 81.1 us -> 81.3 us (level)
  waiting for transfers between devices: 3.34 us -> 0.01 us
  Pallas kernels: 65.3 us -> 68 us
  starting transfers between devices: 3.07 us -> 5.13 us
  local copies, waits for them, and re-layouts: 8.24 us -> 6.36 us
    pallas_call x2 -> x4, Pallas kernels: 34.6 us -> 47.4 us  [segment_maps(): pl.pallas_call(functools.partial(segment_kernel, seqs, dim), grid_spec=pl...]
    pallas_call x1, Pallas kernels: 30.7 us -> 20.3 us  [exchange(): pl.pallas_call(functools.partial(exchange_kernel, devices, seqs), in_spec...]
    ppermute x1 -> x3, waiting for transfers between devices: 3.34 us -> 0.01 us  [shards(): lax.ppermute(array, 'sp', [(i, i ^ step) for i in range(devices)])]
    unnamed x21 -> x17, local copies, waits for them, and re-layouts: 6.45 us -> 3.41 us
    ppermute x1 -> x3, starting transfers between devices: 3.07 us -> 5.13 us  [shards(): lax.ppermute(array, 'sp', [(i, i ^ step) for i in range(devices)])]
  transfers between devices with their start and end apart: 1 -> 3, of which waited for: 1 -> 0; matrix products, arithmetic and copies ran while one was open for 0% -> 0% of each run, Pallas kernels for 21% -> 45%
where the time goes in v2:
time: 81.3 us; the launch traced here: 81 us
  Pallas kernels  68 us (84%)
  local copies, waits for them, and re-layouts  6.36 us (8%)
  starting transfers between devices  5.13 us (6%)
    pallas_call x4, Pallas kernels, segment_maps(): pl.pallas_call(functools.partial(segment_kernel, seqs, dim), grid_spec=pl...  47.4 us
    pallas_call x1, Pallas kernels, exchange(): pl.pallas_call(functools.partial(exchange_kernel, devices, seqs), in_spec...  20.3 us
    ppermute x3, starting transfers between devices, shards(): lax.ppermute(array, 'sp', [(i, i ^ step) for i in range(devices)])  5.13 us
    unnamed x17, local copies, waits for them, and re-layouts  3.41 us
  transfers between devices with their start and end apart: 3, of which 0 were waited for; matrix products, arithmetic and copies ran while one was open for 0% of the time, Pallas kernels for 45%

profile of v2, /device:TPU:0, one launch (start us, length us, event | category | flops | bytes accessed | tf_op | source)
XLA Modules:
  0.0 81.0 jit_solution(3764256457504474189)
XLA Ops:
  0.7 0.8 dynamic-slice_bitcast_fusion
  1.4 0.7 copy.15.shift_ref
  2.1 0.7 copy.16.rate_ref
  2.7 0.8 constant_dynamic-slice_fusion
  3.5 0.6 maximum_bitcast_fusion.wgd_ref
  4.2 11.7 %shard_map.141 = f32[4,128,256]{2,1,0:T(8,128)} custom-call(s32[1]{0:T(128)} %bitcast.9.first_ref, bf16[1024,2048]{1,0:T(8,128)(2,1)} %bitcast.33, bf16[2048,1024]{1,0:T(8,128)(2,1)} %wk_ref.7, bf16[2048,1024]{1,0:T(8,128)(2,1)} %wv_ref.7, bf16[16,2048]{1,0:T(8,128)(2,1)} %maximum_bitcast_fusion.wgd_ref, f32[8,1]{1,0:T(8,128)} %copy.15.shift_ref, ...), custom_call_target="tpu_custom_call" | custom-call | flops 4294967296 | bytes 6291456 | tf_op jit(solution)/shard_map/pallas_call | solution.py:213
  15.9 3.0 %collective-permute-start = (f32[4,128,256]{2,1,0:T(8,128)}, f32[4,128,256]{2,1,0:T(8,128)S(1)}, u32[]{:S(2)}, u32[]{:S(2)}) collective-permute-start(f32[4,128,256]{2,1,0:T(8,128)} %shard_map.141), channel_id=1, source_target_pairs={{0,2},{2,0},{4,6},{6,4},{8,10},{10,8},{12,14},{14,12},{1,3},{3,1},... | collective-permute-start | bytes 1572872 | tf_op jit(solution)/shard_map/ppermute | solution.py:474
  18.9 0.0 copy-start.3
  18.9 0.0 copy-start.4
  18.9 11.9 %shard_map.144 = f32[4,128,256]{2,1,0:T(8,128)} custom-call(s32[1]{0:T(128)} %bitcast.11.first_ref, bf16[1024,2048]{1,0:T(8,128)(2,1)} %bitcast.34, bf16[2048,1024]{1,0:T(8,128)(2,1)} %wk_ref.7, bf16[2048,1024]{1,0:T(8,128)(2,1)} %wv_ref.7, bf16[16,2048]{1,0:T(8,128)(2,1)} %maximum_bitcast_fusion.wgd_ref, f32[8,1]{1,0:T(8,128)} %copy.15.shift_ref, ...), custom_call_target="tpu_custom_call" | custom-call | flops 4294967296 | bytes 6291456 | tf_op jit(solution)/shard_map/pallas_call | solution.py:213
  30.8 0.0 collective-permute-start.1
  30.8 0.0 copy-done.3
  30.8 0.0 copy-done.4
  30.9 0.0 copy-start.5
  30.9 0.0 copy-start.6
  30.9 11.8 %shard_map.140.mine_ref = f32[4,128,256]{2,1,0:T(8,128)} custom-call(s32[1]{0:T(128)} %bitcast.3.first_ref, bf16[1024,2048]{1,0:T(8,128)(2,1)} %bitcast.35, bf16[2048,1024]{1,0:T(8,128)(2,1)} %wk_ref.7, bf16[2048,1024]{1,0:T(8,128)(2,1)} %wv_ref.7, bf16[16,2048]{1,0:T(8,128)(2,1)} %maximum_bitcast_fusion.wgd_ref, f32[8,1]{1,0:T(8,128)} %copy.15.shift_ref, ...), custom_call_target="tpu_custom_call" | custom-call | flops 4294967296 | bytes 6291456 | tf_op jit(solution)/shard_map/pallas_call | solution.py:213
  42.6 0.0 collective-permute-done.theirs_ref
  42.6 0.0 copy-start.1
  42.6 1.0 %copy-done.1 = f32[4,128,256]{2,1,0:T(8,128)S(1)} copy-done((f32[4,128,256]{2,1,0:T(8,128)S(1)}, f32[4,128,256]{2,1,0:T(8,128)}, u32[]{:S(2)}) %copy-start.1) | copy-done | bytes 524312
  43.7 0.4 shard_map.142
  44.1 2.1 %collective-permute-start.2 = (f32[4,128,256]{2,1,0:T(8,128)S(1)}, f32[4,128,256]{2,1,0:T(8,128)S(1)}, u32[]{:S(2)}, u32[]{:S(2)}) collective-permute-start(f32[4,128,256]{2,1,0:T(8,128)S(1)} %shard_map.142), channel_id=1, source_target_pairs={{0,4},{2,6},{4,0},{6,2},{8,12},{10,14},{12,8},{14,10},{1,5},{3,7},... | collective-permute-start | bytes 1572872 | tf_op jit(solution)/shard_map/ppermute | solution.py:474
  46.2 0.0 copy-done.5
  46.3 0.0 copy-done.6
  46.3 0.1 copy.26
  46.4 0.1 broadcast_in_dim.37
  46.5 0.0 copy-start.2
  46.5 12.0 %shard_map.143.ab_ref = f32[4,128,256]{2,1,0:T(8,128)} custom-call(s32[1]{0:T(128)} %bitcast.first_ref, bf16[1024,2048]{1,0:T(8,128)(2,1)} %bitcast.36, bf16[2048,1024]{1,0:T(8,128)(2,1)} %wk_ref.7, bf16[2048,1024]{1,0:T(8,128)(2,1)} %wv_ref.7, bf16[16,2048]{1,0:T(8,128)(2,1)} %maximum_bitcast_fusion.wgd_ref, f32[8,1]{1,0:T(8,128)} %copy.15.shift_ref, ...), custom_call_target="tpu_custom_call" | custom-call | flops 4294967296 | bytes 6291456 | tf_op jit(solution)/shard_map/pallas_call | solution.py:213
  58.4 0.0 collective-permute-done.1.other_ref
  58.4 0.0 collective-permute-done.2.next_ref
  58.5 0.0 copy-done.2
  58.5 0.0 copy-start
  58.5 1.0 %copy-done = f32[4,128,256]{2,1,0:T(8,128)S(1)} copy-done((f32[4,128,256]{2,1,0:T(8,128)S(1)}, f32[4,128,256]{2,1,0:T(8,128)}, u32[]{:S(2)}) %copy-start) | copy-done | bytes 524312
  59.5 20.3 %shard_map.145 = (bf16[2,8,16,128]{3,2,1,0:T(8,128)(2,1)S(1)}, bf16[2,8,128]{2,1,0:T(8,128)(2,1)S(1)}) custom-call(f32[4,128,256]{2,1,0:T(8,128)S(1)} %copy-done, f32[4,128,256]{2,1,0:T(8,128)S(1)} %collective-permute-done.1.other_ref, f32[4,128,256]{2,1,0:T(8,128)S(1)} %collective-permute-done.2.next_ref, f32[16,4,128]{2,1,0:T(4,128)S(1)} %pad_maximum_fusion.info_ref, ...), custom_call_target="tpu_custom_call" | custom-call | tf_op jit(solution)/shard_map/pallas_call | solution.py:400
  79.8 0.6 copy.29
  80.4 0.6 copy.30
  (7 shorter events, 0.1 us)
Async XLA Ops:
  15.9 26.8 %collective-permute-start = (f32[4,128,256]{2,1,0:T(8,128)}, f32[4,128,256]{2,1,0:T(8,128)S(1)}, u32[]{:S(2)}, u32[]{:S(2)}) collective-permute-start(f32[4,128,256]{2,1,0:T(8,128)} %shard_map.141), channel_id=1, source_target_pairs={{0,2},{2,0},{4,6},{6,4},{8,10},{10,8},{12,14},{14,12},{1,3},{3,1},... | collective-permute-start | bytes 1572872 | tf_op jit(solution)/shard_map/ppermute | solution.py:474
  18.9 12.0 %copy-start.3 = (bf16[2,8,128]{2,1,0:T(8,128)(2,1)S(1)}, bf16[2,8,128]{2,1,0:T(8,128)(2,1)}, u32[]{:S(2)}) copy-start(bf16[2,8,128]{2,1,0:T(8,128)(2,1)} %param.21) | copy-start | bytes 12292
  18.9 12.0 %copy-start.4 = (bf16[2,8,128]{2,1,0:T(8,128)(2,1)S(1)}, bf16[2,8,128]{2,1,0:T(8,128)(2,1)}, u32[]{:S(2)}) copy-start(bf16[2,8,128]{2,1,0:T(8,128)(2,1)} %param.22) | copy-start | bytes 12292
  30.8 27.6 %collective-permute-start.1 = (f32[4,128,256]{2,1,0:T(8,128)}, f32[4,128,256]{2,1,0:T(8,128)S(1)}, u32[]{:S(2)}, u32[]{:S(2)}) collective-permute-start(f32[4,128,256]{2,1,0:T(8,128)} %shard_map.144), channel_id=1, source_target_pairs={{0,2},{2,0},{4,6},{6,4},{8,10},{10,8},{12,14},{14,12},{1,3},{3,1},... | collective-permute-start | bytes 1572872 | tf_op jit(solution)/shard_map/ppermute | solution.py:474
  30.9 15.4 %copy-start.5 = (bf16[2,8,128]{2,1,0:T(8,128)(2,1)S(1)}, bf16[2,8,128]{2,1,0:T(8,128)(2,1)}, u32[]{:S(2)}) copy-start(bf16[2,8,128]{2,1,0:T(8,128)(2,1)} %param.23) | copy-start | bytes 12292
  30.9 15.4 %copy-start.6 = (f32[2,8]{1,0:T(2,128)S(1)}, f32[2,8]{1,0:T(2,128)}, u32[]{:S(2)}) copy-start(f32[2,8]{1,0:T(2,128)} %param.24) | copy-start | bytes 196
  42.6 1.0 %copy-start.1 = (f32[4,128,256]{2,1,0:T(8,128)S(1)}, f32[4,128,256]{2,1,0:T(8,128)}, u32[]{:S(2)}) copy-start(f32[4,128,256]{2,1,0:T(8,128)} %shard_map.140.mine_ref) | copy-start | bytes 1572868
  44.1 14.4 %collective-permute-start.2 = (f32[4,128,256]{2,1,0:T(8,128)S(1)}, f32[4,128,256]{2,1,0:T(8,128)S(1)}, u32[]{:S(2)}, u32[]{:S(2)}) collective-permute-start(f32[4,128,256]{2,1,0:T(8,128)S(1)} %shard_map.142), channel_id=1, source_target_pairs={{0,4},{2,6},{4,0},{6,2},{8,12},{10,14},{12,8},{14,10},{1,5},{3,7},... | collective-permute-start | bytes 1572872 | tf_op jit(solution)/shard_map/ppermute | solution.py:474
  46.5 12.0 %copy-start.2 = (f32[128]{0:T(128)S(1)}, f32[128]{0:T(128)}, u32[]{:S(2)}) copy-start(f32[128]{0:T(128)} %param.25) | copy-start | bytes 1540
  58.5 1.0 %copy-start = (f32[4,128,256]{2,1,0:T(8,128)S(1)}, f32[4,128,256]{2,1,0:T(8,128)}, u32[]{:S(2)}) copy-start(f32[4,128,256]{2,1,0:T(8,128)} %shard_map.143.ab_ref) | copy-start | bytes 1572868
